TPU v7x, 256 devices: a 4x2x16 block of a 4x16x16 slice. The times are simulated.
256 devices in a mesh: grp: 2 (over y), ep: 64 (over z, x), tp: 2 (over core).
Axes of the slice: x: 4, y: 2, z: 16, core: 2. Of those that a mesh axis runs over, the one named last changes fastest.
The devices are a block of a 4x16x16 slice.
Arguments:
- tokens: bfloat16 [16384, 2048], P(('grp', 'ep')), parts along dimension 0, may hold values from -6 to 6
- in_gain: float32 [2048], replicated, may hold values from 0.1 to 1.9
- routing: int32 [16384, 4], P(('grp', 'ep')), parts along dimension 0, may hold values from 0 to 127, as said below
- gate_prob: float32 [16384, 4], P(('grp', 'ep')), parts along dimension 0, may hold values from 0.05 to 1
- w_gate: bfloat16 [128, 2048, 512], P('ep', None, 'tp'), may hold values from -0.125 to 0.125
- w_up: bfloat16 [128, 2048, 512], P('ep', None, 'tp'), may hold values from -0.125 to 0.125
- w_down: bfloat16 [128, 512, 2048], P('ep', 'tp')
- out_gain: float32 [2048], P('tp'), may hold values from 0.1 to 1.9
Outputs:
- output: bfloat16 [16384, 2048], P(('grp', 'ep'), 'tp'), parts along dimension 0
There are 2 independent parts, one for each index of `grp`. A program takes and returns all parts, laid end to end along the dimension named above; an argument that names none is the same for every part. Nothing has to cross between parts.
Inputs may be any that keep to these rules, and one draw needn't show every extreme that they name: `routing`: each row names 4 different experts, all of one group (the same value of expert // 32). In the rows of one device no expert is named more than 8 times, and in every device's rows some expert is named exactly 8 times.
All inputs are finite; a program needn't handle non-finite values.
Results may differ from a plain program's by a relative error of at most 0.0077.
Values may be sent and summed in bfloat16 or wider, within the bound.
A program may use at most 64 MiB of HBM per device.

v0:
```python
import jax
import jax.numpy as jnp
from jax import lax
from jax.sharding import PartitionSpec as P

GROUPS = 4
EPS = 1e-06


def split_up(value, dim, peers):
    dims = value.shape
    tiles = value.reshape(*dims[:dim], peers, dims[dim] // peers, *dims[dim + 1 :])
    return jnp.moveaxis(tiles, dim, 0)


def sent_and_summed(value, axis, dim):
    tiles = split_up(value, dim, lax.axis_size(axis))
    arrived = lax.all_to_all(tiles, axis, split_axis=0, concat_axis=0, tiled=True)
    return arrived.astype(jnp.float32).sum(axis=0)


def gathered_total(value, axis):
    tiles = lax.all_gather(value, axis)
    return tiles.sum(axis=0)


def slot_ranks(flat_routes, expert_count):
    matches = (flat_routes[:, None] == jnp.arange(expert_count, dtype=jnp.int32)[None, :]).astype(
        jnp.int32
    )
    earlier = jnp.cumsum(matches, axis=0) - matches
    return jnp.sum(earlier * matches, axis=1)


def fill_rows(source, entries):
    filled = entries > 0
    return jnp.where(
        filled[:, None], source[jnp.maximum(entries - 1, 0)], jnp.zeros((), source.dtype)
    )


def body(tokens, in_gain, routing, gate_prob, w_gate, w_up, w_down, out_gain):
    ep_count = lax.axis_size("ep")
    local_experts = w_gate.shape[0]
    expert_count = local_experts * ep_count
    tok_dev, top_count = routing.shape
    model_width = tokens.shape[1]
    half_width = out_gain.shape[0]
    group_width = expert_count // GROUPS
    row_cap = max(2, tok_dev * top_count // (2 * group_width))
    floats = tokens.astype(jnp.float32)
    normed = (
        floats * lax.rsqrt(jnp.mean(floats * floats, axis=-1, keepdims=True) + EPS) * in_gain
    ).astype(jnp.bfloat16)
    flat_routes = routing.reshape(-1)
    slot_rank = slot_ranks(flat_routes, expert_count)
    slot_ids = flat_routes * row_cap + slot_rank
    token_ids = jnp.arange(tok_dev * top_count, dtype=jnp.int32) // top_count
    slot_table = jnp.zeros((expert_count * row_cap,), jnp.int32).at[slot_ids].set(token_ids + 1)
    own_columns = lax.dynamic_slice_in_dim(normed, lax.axis_index("tp") * half_width, half_width, 1)
    sendbuf = fill_rows(own_columns, slot_table).reshape(
        ep_count, local_experts, row_cap, half_width
    )
    arrived = lax.all_to_all(sendbuf, "ep", split_axis=0, concat_axis=0, tiled=True)
    arrived = lax.all_gather(arrived, "tp", axis=3, tiled=True)
    gate_act = jnp.einsum("secd,edf->secf", arrived, w_gate, preferred_element_type=jnp.float32)
    up_act = jnp.einsum("secd,edf->secf", arrived, w_up, preferred_element_type=jnp.float32)
    hidden = (jax.nn.silu(gate_act) * up_act).astype(jnp.bfloat16)
    partial_out = jnp.einsum("secf,efd->secd", hidden, w_down, preferred_element_type=jnp.float32)
    results = sent_and_summed(partial_out.astype(jnp.bfloat16), "tp", 3).astype(jnp.bfloat16)
    returned = lax.all_to_all(results, "ep", split_axis=0, concat_axis=0, tiled=True).reshape(
        expert_count * row_cap, half_width
    )
    picked = returned[slot_ids].astype(jnp.float32).reshape(tok_dev, top_count, half_width)
    mixed_rows = jnp.sum(picked * gate_prob[:, :, None], axis=1)
    squares = jnp.sum(mixed_rows * mixed_rows, axis=1)
    total_squares = gathered_total(squares, "tp")
    inv_rms = lax.rsqrt(total_squares / model_width + EPS)
    return (mixed_rows * inv_rms[:, None] * out_gain).astype(jnp.bfloat16)


def solution(mesh):
    placed = (
        P(("grp", "ep"), None),
        P(),
        P(("grp", "ep"), None),
        P(("grp", "ep"), None),
        P("ep", None, "tp"),
        P("ep", None, "tp"),
        P("ep", "tp", None),
        P("tp"),
    )
    return jax.shard_map(
        body, mesh=mesh, in_specs=placed, out_specs=P(("grp", "ep"), "tp"), check_vma=False
    )
```

profile of v0, /device:TPU:33, one launch (start us, length us, event | category | flops | bytes accessed | tf_op | source)
XLA Modules:
  0.0 331.5 jit_solution(8232878903041759823)
XLA Ops:
  6.5 0.0 copy-start
  6.6 0.0 copy-start.1
  6.6 0.0 all-gather.4.cloned.1.call-start
  6.6 0.0 copy-start.4
  6.6 1.3 convert_element_type.36
  7.9 1.2 multiply_reduce_fusion.1
  9.1 0.0 copy-done.1
  9.1 0.1 copy.29
  9.2 0.1 eq.29
  9.3 0.1 eq.25
  9.4 0.1 copy.31
  9.6 0.2 fusion.24
  9.9 0.1 copy.28
  10.0 0.1 mul.77
  10.1 0.2 fusion.23
  10.3 2.4 scatter_custom_fusion
  12.8 0.1 broadcast_in_dim.16
  13.0 0.0 copy-done.4
  13.0 0.1 fusion.20
  13.1 5.4 %gather_fusion = bf16[1024,1024]{1,0:T(8,128)(2,1)} fusion(bf16[128,1024]{1,0:T(8,128)(2,1)S(1)} %fusion.20, s32[1024]{0:T(1024)S(1)} %maximum_clamp_fusion), kind=kCustom, calls=%fused_computation | custom fusion | bytes 4198400 | tf_op jit(solution)/shard_map/gather | solution.py:38
  18.5 1.8 broadcast_select_fusion
  20.3 124.6 %all_to_all.15 = bf16[64,2,8,1024]{3,2,1,0:T(8,128)(2,1)S(1)} all-to-all(bf16[64,2,8,1024]{3,2,1,0:T(8,128)(2,1)S(1)} %broadcast_select_fusion), channel_id=1, replica_groups=mesh['grp'=2,'ep'=64,'tp'=2] {'ep'}, dimensions={0} | all-to-all | bytes 4194304 | tf_op jit(solution)/shard_map/all_to_all | solution.py:64
  144.9 1.5 copy.33
  146.4 0.1 all-gather.4.cloned.1.call-update
  146.5 19.9 %all-gather.4.cloned.1.call-done = bf16[64,2,8,2048]{3,2,0,1:T(8,128)(2,1)} async-done(((bf16[64,2,8,1024]{3,2,0,1:T(8,128)(2,1)}), bf16[64,2,8,2048]{3,2,0,1:T(8,128)(2,1)}) %all-gather.4.cloned.1.call-update) | async-done | bytes 4194320 | tf_op jit(solution)/shard_map/all_gather | solution.py:65
  166.4 4.1 %fusion.5 = f32[64,2,8,256]{3,2,0,1:T(8,128)S(1)} fusion(bf16[64,2,8,2048]{3,2,0,1:T(8,128)(2,1)} %all-gather.4.cloned.1.call-done, bf16[2,2048,256]{2,1,0:T(8,128)(2,1)} %param.12), kind=kOutput, calls=%fused_computation.12 | convolution fusion | flops 1073741824 | bytes 7340032 | tf_op jit(solution)/shard_map/secd,edf->secf/dot_general | solution.py:66
  170.5 0.0 copy-done
  170.5 7.2 %convolution_convert_fusion = bf16[2,64,8,2048]{3,2,1,0:T(8,128)(2,1)} fusion(bf16[2,256,2048]{2,1,0:T(8,128)(2,1)S(1)} %copy-done, bf16[64,2,8,2048]{3,2,0,1:T(8,128)(2,1)} %all-gather.4.cloned.1.call-done, bf16[2,2048,256]{2,1,0:T(8,128)(2,1)} %param.13, f32[64,2,8,256]{3,2,0,1:T(8,128)S(1)} %fusion.5), kind=kOutput, calls=%fused_computation.4 | convolution fusion | flops 2151153664 | bytes 13631488 | tf_op jit(solution)/shard_map/secf,efd->secd/dot_general | solution.py:69
  177.7 2.6 copy.43
  180.4 8.0 %all_to_all.16 = bf16[2,64,2,8,1024]{4,3,1,2,0:T(8,128)(2,1)} all-to-all(bf16[2,64,2,8,1024]{4,3,1,2,0:T(8,128)(2,1)S(1)} %bitcast.61), channel_id=1, replica_groups=mesh['grp'=2,'ep'=64,'tp'=2] {'tp'}, dimensions={0} | all-to-all | bytes 8388608 | tf_op jit(solution)/shard_map/all_to_all | solution.py:18
  188.4 5.2 %reduce_sum.62 = bf16[64,2,8,1024]{3,2,0,1:T(8,128)(2,1)} reduce(bf16[2,64,2,8,1024]{4,3,1,2,0:T(8,128)(2,1)} %all_to_all.16, bf16[]{:T(256)} %constant.55.clone.1), dimensions={0}, to_apply=%region_5.6 | reduce | flops 1048576 | bytes 6291458 | tf_op jit(solution)/shard_map/reduce_sum | solution.py:19
  193.6 3.2 copy.36
  196.8 0.0 copy-start.3
  196.8 16.3 %all-to-all-start.2 = ((bf16[64,2,8,1024]{3,2,1,0:T(8,128)(2,1)}), bf16[64,2,8,1024]{3,2,1,0:T(8,128)(2,1)}, u32[]{:S(2)}, u32[]{:S(2)}) async-start(bf16[64,2,8,1024]{3,2,1,0:T(8,128)(2,1)} %copy.36), calls=%async_computation.2 | async-start | bytes 4194304 | tf_op jit(solution)/shard_map/all_to_all | solution.py:71
  213.1 0.0 copy-done.3
  213.1 0.1 copy.37
  213.2 95.1 %all-to-all-done.2 = bf16[64,2,8,1024]{3,2,1,0:T(8,128)(2,1)} async-done(((bf16[64,2,8,1024]{3,2,1,0:T(8,128)(2,1)}), bf16[64,2,8,1024]{3,2,1,0:T(8,128)(2,1)}, u32[]{:S(2)}, u32[]{:S(2)}) %all-to-all-start.2) | async-done | bytes 2097184 | tf_op jit(solution)/shard_map/all_to_all | solution.py:71
  308.3 4.6 %gather_fusion.1 = bf16[512,1024]{1,0:T(8,128)(2,1)S(1)} fusion(bf16[1024,1024]{1,0:T(8,128)(2,1)} %bitcast.17, s32[1024]{0:T(1024)S(1)} %pad_clamp_fusion), kind=kCustom, calls=%fused_computation.1 | custom fusion | bytes 2099200 | tf_op jit(solution)/shard_map/gather | solution.py:74
  312.9 1.7 reshape.83
  314.6 0.0 copy-start.2
  314.6 3.0 multiply_reduce_fusion
  317.6 0.1 multiply_reduce_fusion.2
  317.7 6.1 %all-gather.1 = f32[2,1,128]{2,1,0:T(1,128)S(1)} all-gather(f32[1,1,128]{2,1,0:T(1,128)S(1)} %bitcast.70), channel_id=2, replica_groups=mesh['grp'=2,'ep'=64,'tp'=2] {'tp'}, dimensions={0}, use_global_device_ids=true | all-gather | bytes 1536 | tf_op jit(solution)/shard_map/all_gather | solution.py:23
  323.9 0.0 copy-done.2
  323.9 0.8 multiply_convert_fusion
  (16 shorter events, 0.2 us)
Async XLA Ops:
  6.5 164.0 %copy-start = (bf16[2,256,2048]{2,1,0:T(8,128)(2,1)S(1)}, bf16[2,256,2048]{2,1,0:T(8,128)(2,1)}, u32[]{:S(2)}) copy-start(bf16[2,256,2048]{2,1,0:T(8,128)(2,1)} %param.14) | copy-start | bytes 6291460
  6.6 2.5 copy-start.1
  6.6 159.8 %all-gather.4.cloned.1.call-start = ((), (), s32[]{:S(2)}) async-start(), calls=%async_computation.3 | async-start | bytes 6291456 | tf_op jit(solution)/shard_map/all_gather | solution.py:65
  6.6 6.4 %copy-start.4 = (f32[2048]{0:T(1024)S(1)}, f32[2048]{0:T(1024)}, u32[]{:S(2)}) copy-start(f32[2048]{0:T(1024)} %param.9) | copy-start | bytes 24580
  196.8 16.3 %copy-start.3 = (f32[128,4]{0,1:T(4,128)S(1)}, f32[128,4]{0,1:T(4,128)}, u32[]{:S(2)}) copy-start(f32[128,4]{0,1:T(4,128)} %param.11) | copy-start | bytes 6148
  196.8 111.5 %all-to-all-start.2 = ((bf16[64,2,8,1024]{3,2,1,0:T(8,128)(2,1)}), bf16[64,2,8,1024]{3,2,1,0:T(8,128)(2,1)}, u32[]{:S(2)}, u32[]{:S(2)}) async-start(bf16[64,2,8,1024]{3,2,1,0:T(8,128)(2,1)} %copy.36), calls=%async_computation.2 | async-start | bytes 4194304 | tf_op jit(solution)/shard_map/all_to_all | solution.py:71
  314.6 9.2 %copy-start.2 = (f32[1024]{0:T(1024)S(1)}, f32[1024]{0:T(1024)}, u32[]{:S(2)}) copy-start(f32[1024]{0:T(1024)} %param.15) | copy-start | bytes 12292
Sparse Core Ops, SparseCore 0:
  146.6 19.7 all-gather.3
where the time goes:
time: 332 us
  blocking collectives  139 us (42%)
  waiting for transfers between devices  115 us (35%)
  local copies, waits for them, and re-layouts  22.4 us (7%)
  starting transfers between devices  16.3 us (5%)
  other arithmetic  14.1 us (4%)
  between operations  13.6 us (4%)
  matrix products  11.3 us (3%)
    all_to_all x1, blocking collectives, body(): lax.all_to_all(sendbuf, 'ep', split_axis=0, concat_axis=0, tiled=True)  125 us
    all_to_all x1, waiting for transfers between devices, body(): lax.all_to_all(results, 'ep', split_axis=0, concat_axis=0, tiled=True)  95.1 us
    all_gather x1, waiting for transfers between devices, body(): arrived = lax.all_gather(arrived, 'tp', axis=3, tiled=True)  19.9 us
    all_to_all x1, starting transfers between devices, body(): lax.all_to_all(results, 'ep', split_axis=0, concat_axis=0, tiled=True)  16.3 us
    all_to_all x1, blocking collectives, sent_and_summed(): lax.all_to_all(tiles, axis, split_axis=0, concat_axis=0, tiled=True)  8.04 us
    dot_general x1, matrix products, body(): jnp.einsum('secf,efd->secd', hidden, w_down, preferred_element_type=jnp.f...  7.24 us
  transfers between devices with their start and end apart: 2, of which 2 were waited for; matrix products, arithmetic and copies ran while one was open for 0% of the time, Pallas kernels for 0%

commit v1 on v0

--- a/solution.py
+++ b/solution.py
@@ -62,7 +62,11 @@
         ep_count, local_experts, row_cap, half_width
     )
     arrived = lax.all_to_all(sendbuf, "ep", split_axis=0, concat_axis=0, tiled=True)
-    arrived = lax.all_gather(arrived, "tp", axis=3, tiled=True)
+    size = lax.axis_size("tp")
+    repeats = [size if d == 3 else 1 for d in range(arrived.ndim)]
+    arrived = lax.all_to_all(
+        jnp.tile(arrived, repeats), "tp", split_axis=3, concat_axis=3, tiled=True
+    )
     gate_act = jnp.einsum("secd,edf->secf", arrived, w_gate, preferred_element_type=jnp.float32)
     up_act = jnp.einsum("secd,edf->secf", arrived, w_up, preferred_element_type=jnp.float32)
     hidden = (jax.nn.silu(gate_act) * up_act).astype(jnp.bfloat16)

time: 332 us -> 351 us (1.057)
  local copies, waits for them, and re-layouts: 22.4 us -> 67.3 us
  waiting for transfers between devices: 115 us -> 94.9 us
  blocking collectives: 139 us -> 155 us
  between operations: 13.6 us -> 0.21 us
  starting transfers between devices: 16.3 us -> 7.55 us
    all_gather x1 -> x0, waiting for transfers between devices: 19.9 us -> none  [body(): arrived = lax.all_gather(arrived, 'tp', axis=3, tiled=True)]
    unnamed x13 -> x15, local copies, waits for them, and re-layouts: 0.25 us -> 20 us
    all_to_all x0 -> x1, blocking collectives: none -> 16.1 us  [body(): lax.all_to_all(jnp.tile(arrived, repeats), 'tp', split_axis=3, concat_axi...]
    all_to_all x0 -> x1, local copies, waits for them, and re-layouts: none -> 12 us  [body(): lax.all_to_all(jnp.tile(arrived, repeats), 'tp', split_axis=3, concat_axi...]
    all_to_all x1, starting transfers between devices: 16.3 us -> 7.55 us  [body(): lax.all_to_all(results, 'ep', split_axis=0, concat_axis=0, tiled=True)]
    all_to_all x1, local copies, waits for them, and re-layouts: 1.52 us -> 8.17 us  [body(): lax.all_to_all(sendbuf, 'ep', split_axis=0, concat_axis=0, tiled=True)]
    another operation x3 -> x4, local copies, waits for them, and re-layouts: 0.03 us -> 6.51 us  [the longest x1 6.49 us: body(): jnp.tile(arrived, repeats)]
  transfers between devices with their start and end apart: 2 -> 1, of which waited for: 2 -> 1; matrix products, arithmetic and copies ran while one was open for 0% -> 0% of each run, Pallas kernels for 0% -> 0%
where the time goes in v1:
time: 351 us; the launch traced here: 350 us
  blocking collectives  155 us (44%)
  waiting for transfers between devices  94.9 us (27%)
  local copies, waits for them, and re-layouts  67.3 us (19%)
  other arithmetic  14.1 us (4%)
  matrix products  11.3 us (3%)
  starting transfers between devices  7.55 us (2%)
    all_to_all x1, blocking collectives, body(): lax.all_to_all(sendbuf, 'ep', split_axis=0, concat_axis=0, tiled=True)  125 us
    all_to_all x1, waiting for transfers between devices, body(): lax.all_to_all(results, 'ep', split_axis=0, concat_axis=0, tiled=True)  94.9 us
    unnamed x15, local copies, waits for them, and re-layouts  20 us
    all_to_all x1, blocking collectives, body(): lax.all_to_all(jnp.tile(arrived, repeats), 'tp', split_axis=3, concat_axi...  16.1 us
    all_to_all x1, local copies, waits for them, and re-layouts, body(): lax.all_to_all(jnp.tile(arrived, repeats), 'tp', split_axis=3, concat_axi...  12 us
    all_to_all x1, local copies, waits for them, and re-layouts, body(): lax.all_to_all(sendbuf, 'ep', split_axis=0, concat_axis=0, tiled=True)  8.17 us
    all_to_all x1, blocking collectives, sent_and_summed(): lax.all_to_all(tiles, axis, split_axis=0, concat_axis=0, tiled=True)  8.12 us
    all_to_all x1, starting transfers between devices, body(): lax.all_to_all(results, 'ep', split_axis=0, concat_axis=0, tiled=True)  7.55 us
  transfers between devices with their start and end apart: 1, of which 1 were waited for; matrix products, arithmetic and copies ran while one was open for 0% of the time, Pallas kernels for 0%

profile of v1, /device:TPU:33, one launch (start us, length us, event | category | flops | bytes accessed | tf_op | source)
XLA Modules:
  0.0 350.4 jit_solution(2604830941224924054)
XLA Ops:
  0.0 0.0 copy-start
  0.0 0.0 copy-start.1
  0.0 0.0 copy-start.4
  0.0 1.3 convert_element_type.36
  1.3 1.2 multiply_reduce_fusion.1
  2.5 0.0 copy-done.1
  2.5 0.1 copy.31
  2.6 0.1 eq.29
  2.8 0.1 eq.25
  2.9 0.1 copy.33
  3.0 0.2 fusion.24
  3.3 0.1 copy.30
  3.4 0.1 mul.77
  3.5 0.2 fusion.23
  3.8 2.4 scatter_custom_fusion
  6.3 0.1 broadcast_in_dim.16
  6.4 0.0 copy-done.4
  6.4 0.1 fusion.20
  6.6 5.4 %gather_fusion = bf16[1024,1024]{1,0:T(8,128)(2,1)} fusion(bf16[128,1024]{1,0:T(8,128)(2,1)S(1)} %fusion.20, s32[1024]{0:T(1024)S(1)} %maximum_clamp_fusion), kind=kCustom, calls=%fused_computation | custom fusion | bytes 4198400 | tf_op jit(solution)/shard_map/gather | solution.py:38
  11.9 1.8 broadcast_select_fusion
  13.7 124.7 %all_to_all.20 = bf16[64,2,8,1024]{3,2,1,0:T(8,128)(2,1)} all-to-all(bf16[64,2,8,1024]{3,2,1,0:T(8,128)(2,1)S(1)} %broadcast_select_fusion), channel_id=1, replica_groups=mesh['grp'=2,'ep'=64,'tp'=2] {'ep'}, dimensions={0} | all-to-all | bytes 4194304 | tf_op jit(solution)/shard_map/all_to_all | solution.py:64
  138.4 8.2 %copy.35 = bf16[64,2,8,1024]{0,2,1,3:T(8,128)(2,1)} copy(bf16[64,2,8,1024]{3,2,1,0:T(8,128)(2,1)} %all_to_all.20) | data formatting | bytes 4194304 | tf_op jit(solution)/shard_map/all_to_all | solution.py:64
  146.6 6.5 %tile.4 = bf16[64,2,8,2,1024]{0,2,1,4,3:T(8,128)(2,1)} broadcast(bf16[64,2,8,1024]{0,2,1,3:T(8,128)(2,1)} %copy.35), dimensions={0,1,2,4} | broadcast | bytes 6291456 | tf_op jit(solution)/shard_map/tile | solution.py:68
  153.1 10.0 %reshape.122 = bf16[2,2,524288]{2,1,0:T(2,128)(2,1)} reshape(bf16[2048,2,8,64]{3,2,1,0:T(8,128)(2,1)} %bitcast.64) | data formatting | bytes 8388608
  163.1 16.1 %all_to_all.21 = bf16[2,2,524288]{2,1,0:T(2,128)(2,1)} all-to-all(bf16[2,2,524288]{2,1,0:T(2,128)(2,1)} %reshape.122), channel_id=1, replica_groups=mesh['grp'=2,'ep'=64,'tp'=2] {'tp'}, dimensions={0} | all-to-all | bytes 8388608 | tf_op jit(solution)/shard_map/all_to_all | solution.py:67
  179.2 9.8 %reshape.123 = bf16[2048,2,8,64]{3,2,1,0:T(8,128)(2,1)} reshape(bf16[2,2,524288]{2,1,0:T(2,128)(2,1)} %all_to_all.21) | data formatting | bytes 8388608
  189.0 12.0 %copy.36 = bf16[64,2,8,2048]{3,2,0,1:T(8,128)(2,1)} copy(bf16[64,2,8,2048]{0,2,1,3:T(8,128)(2,1)} %bitcast.65) | data formatting | bytes 8388608 | tf_op jit(solution)/shard_map/all_to_all | solution.py:67
  201.0 4.1 %fusion.5 = f32[64,2,8,256]{3,2,0,1:T(8,128)S(1)} fusion(bf16[64,2,8,2048]{3,2,0,1:T(8,128)(2,1)} %copy.36, bf16[2,2048,256]{2,1,0:T(8,128)(2,1)} %param.12), kind=kOutput, calls=%fused_computation.12 | convolution fusion | flops 1073741824 | bytes 7340032 | tf_op jit(solution)/shard_map/secd,edf->secf/dot_general | solution.py:70
  205.1 0.0 copy-done
  205.1 7.2 %convolution_convert_fusion = bf16[2,64,8,2048]{3,2,1,0:T(8,128)(2,1)} fusion(bf16[2,256,2048]{2,1,0:T(8,128)(2,1)S(1)} %copy-done, bf16[64,2,8,2048]{3,2,0,1:T(8,128)(2,1)} %copy.36, bf16[2,2048,256]{2,1,0:T(8,128)(2,1)} %param.13, f32[64,2,8,256]{3,2,0,1:T(8,128)S(1)} %fusion.5), kind=kOutput, calls=%fused_computation.4 | convolution fusion | flops 2151153664 | bytes 13631488 | tf_op jit(solution)/shard_map/secf,efd->secd/dot_general | solution.py:73
  212.3 2.6 copy.47
  214.9 8.1 %all_to_all.22 = bf16[2,64,2,8,1024]{4,3,1,2,0:T(8,128)(2,1)} all-to-all(bf16[2,64,2,8,1024]{4,3,1,2,0:T(8,128)(2,1)S(1)} %bitcast.66), channel_id=1, replica_groups=mesh['grp'=2,'ep'=64,'tp'=2] {'tp'}, dimensions={0} | all-to-all | bytes 8388608 | tf_op jit(solution)/shard_map/all_to_all | solution.py:18
  223.1 5.2 %reduce_sum.62 = bf16[64,2,8,1024]{3,2,0,1:T(8,128)(2,1)} reduce(bf16[2,64,2,8,1024]{4,3,1,2,0:T(8,128)(2,1)} %all_to_all.22, bf16[]{:T(256)} %constant.55.clone.1), dimensions={0}, to_apply=%region_5.6 | reduce | flops 1048576 | bytes 6291458 | tf_op jit(solution)/shard_map/reduce_sum | solution.py:19
  228.2 3.2 copy.40
  231.4 0.0 copy-start.3
  231.4 7.5 %all-to-all-start.3 = ((bf16[64,2,8,1024]{3,2,1,0:T(8,128)(2,1)}), bf16[64,2,8,1024]{3,2,1,0:T(8,128)(2,1)}, u32[]{:S(2)}, u32[]{:S(2)}) async-start(bf16[64,2,8,1024]{3,2,1,0:T(8,128)(2,1)} %copy.40), calls=%async_computation.3 | async-start | bytes 4194304 | tf_op jit(solution)/shard_map/all_to_all | solution.py:75
  239.0 0.0 copy-done.3
  239.0 0.1 copy.41
  239.1 94.9 %all-to-all-done.3 = bf16[64,2,8,1024]{3,2,1,0:T(8,128)(2,1)} async-done(((bf16[64,2,8,1024]{3,2,1,0:T(8,128)(2,1)}), bf16[64,2,8,1024]{3,2,1,0:T(8,128)(2,1)}, u32[]{:S(2)}, u32[]{:S(2)}) %all-to-all-start.3) | async-done | bytes 2097184 | tf_op jit(solution)/shard_map/all_to_all | solution.py:75
  334.0 4.6 %gather_fusion.1 = bf16[512,1024]{1,0:T(8,128)(2,1)S(1)} fusion(bf16[1024,1024]{1,0:T(8,128)(2,1)} %bitcast.18, s32[1024]{0:T(1024)S(1)} %pad_clamp_fusion), kind=kCustom, calls=%fused_computation.1 | custom fusion | bytes 2099200 | tf_op jit(solution)/shard_map/gather | solution.py:78
  338.6 1.7 reshape.87
  340.3 0.0 copy-start.2
  340.3 3.0 multiply_reduce_fusion
  343.3 0.1 multiply_reduce_fusion.2
  343.4 6.1 %all-gather.1 = f32[2,1,128]{2,1,0:T(1,128)S(1)} all-gather(f32[1,1,128]{2,1,0:T(1,128)S(1)} %bitcast.75), channel_id=2, replica_groups=mesh['grp'=2,'ep'=64,'tp'=2] {'tp'}, dimensions={0}, use_global_device_ids=true | all-gather | bytes 1536 | tf_op jit(solution)/shard_map/all_gather | solution.py:23
  349.5 0.0 copy-done.2
  349.5 0.8 multiply_convert_fusion
  (16 shorter events, 0.2 us)
Async XLA Ops:
  0.0 205.1 %copy-start = (bf16[2,256,2048]{2,1,0:T(8,128)(2,1)S(1)}, bf16[2,256,2048]{2,1,0:T(8,128)(2,1)}, u32[]{:S(2)}) copy-start(bf16[2,256,2048]{2,1,0:T(8,128)(2,1)} %param.14) | copy-start | bytes 6291460
  0.0 2.5 copy-start.1
  0.0 6.4 %copy-start.4 = (f32[2048]{0:T(1024)S(1)}, f32[2048]{0:T(1024)}, u32[]{:S(2)}) copy-start(f32[2048]{0:T(1024)} %param.9) | copy-start | bytes 24580
  231.4 7.6 %copy-start.3 = (f32[128,4]{0,1:T(4,128)S(1)}, f32[128,4]{0,1:T(4,128)}, u32[]{:S(2)}) copy-start(f32[128,4]{0,1:T(4,128)} %param.11) | copy-start | bytes 6148
  231.4 102.6 %all-to-all-start.3 = ((bf16[64,2,8,1024]{3,2,1,0:T(8,128)(2,1)}), bf16[64,2,8,1024]{3,2,1,0:T(8,128)(2,1)}, u32[]{:S(2)}, u32[]{:S(2)}) async-start(bf16[64,2,8,1024]{3,2,1,0:T(8,128)(2,1)} %copy.40), calls=%async_computation.3 | async-start | bytes 4194304 | tf_op jit(solution)/shard_map/all_to_all | solution.py:75
  340.3 9.2 %copy-start.2 = (f32[1024]{0:T(1024)S(1)}, f32[1024]{0:T(1024)}, u32[]{:S(2)}) copy-start(f32[1024]{0:T(1024)} %param.15) | copy-start | bytes 12292
